TPU v7x, 512 devices: a 4x2x32 block of a 4x8x32 slice. The times are simulated.
512 devices in a mesh: grp: 2 (over y), sp: 32 (over z), tp: 8 (over x, core).
Axes of the slice: x: 4, y: 2, z: 32, core: 2. Of those that a mesh axis runs over, the one named last changes fastest.
The devices are a block of a 4x8x32 slice.
Arguments:
- inputs: bfloat16 [16384, 2048], P(('grp', 'sp'), 'tp'), parts along dimension 0, may hold values from -20 to 20
- norm_gain: bfloat16 [2048], replicated, may hold values from 0.099609375 to 1.8984375
- w_conv_in: bfloat16 [1024, 2048], P('tp'), may hold values from -0.125 to 0.125
- w_conv_gate: bfloat16 [1024, 2048], P('tp'), may hold values from -0.125 to 0.125
- conv_kernel: bfloat16 [31, 1024], P(None, 'tp'), may hold values from -4.3105272 to 4.3105272
- ln_gain: bfloat16 [1024], P('tp'), may hold values from 0.099609375 to 1.8984375
- w_query: bfloat16 [1024, 2048], P('tp'), may hold values from -0.53033009 to 0.53033009
- w_key: bfloat16 [1024, 2048], P('tp'), may hold values from -0.53033009 to 0.53033009
- w_value: bfloat16 [1024, 2048], P('tp'), may hold values from -0.125 to 0.125
- cum_gate: float32 [16, 16384], P('tp', ('grp', 'sp')), parts along dimension 1, may hold values from -8192 to 0, as said below
- w_conv_out: bfloat16 [1024, 2048], P('tp'), may hold values from -0.125 to 0.125
- w_attn_out: bfloat16 [1024, 2048], P('tp'), may hold values from -0.125 to 0.125
Outputs:
- mixed: bfloat16 [16384, 2048], P(('grp', 'sp', 'tp')), parts along dimension 0
- log_total: float32 [16, 16384], P('tp', ('grp', 'sp')), parts along dimension 1
There are 2 independent parts, one for each index of `grp`. A program takes and returns all parts, laid end to end along the dimension named above; an argument that names none is the same for every part. Nothing has to cross between parts.
Inputs may be any that keep to these rules, and one draw needn't show every extreme that they name: cum_gate never rises along positions: entry t is the sum of the head's log forget gates at positions 0 to t.
All inputs are finite; a program needn't handle non-finite values.
Results may differ from a plain program's by a relative error of at most 0.0144.
Values may be sent and summed in bfloat16 or wider, within the bound.
A program may use at most 64 MiB of HBM per device.

v0:
```python
import jax
import jax.numpy as jnp
from jax import lax
from jax.sharding import PartitionSpec as P

D = 2048
CONV_CH = 1024
neg_large = -1e30


def sent_to_all(shard, axis):
    devices = lax.axis_size(axis)
    return lax.all_to_all(
        jnp.broadcast_to(shard[None], (devices, *shard.shape)), axis, 0, 0, tiled=True
    )


def in_order(parts, dim):
    lengths = list(parts.shape[1:])
    lengths[dim] *= parts.shape[0]
    return jnp.moveaxis(parts, 0, dim).reshape(lengths)


def gather_directly(shard, axis, dim):
    parts = sent_to_all(shard, axis)
    return in_order(parts, dim)


def passed_along(block, axis, distance):
    devices = range(lax.axis_size(axis))
    route = [(i - distance, i) for i in devices if i - distance in devices]
    return lax.ppermute(block, axis, route)


def sent_together(arrays, axis, dim, along):
    both = jnp.concatenate(arrays, axis=along)
    filled, at, outs = (lax.all_gather(both, axis, axis=dim, tiled=True), 0, [])
    for a in arrays:
        outs.append(lax.slice_in_dim(filled, at, at + a.shape[along], axis=along))
        at += a.shape[along]
    return tuple(outs)


def in_blocks(shard, dim, devices):
    lengths = shard.shape
    parts = shard.reshape(*lengths[:dim], devices, lengths[dim] // devices, *lengths[dim + 1 :])
    return jnp.moveaxis(parts, dim, 0)


def summed_on_arrival(shard, axis, dim):
    devices = lax.axis_size(axis)
    parts = lax.all_to_all(in_blocks(shard, dim, devices), axis, 0, 0, tiled=True)
    return jnp.sum(parts.astype(jnp.float32), axis=0)


def block_terms(q_blk, q_cum, k_blk, v_blk, k_cum, q_first, k_first):
    score_scale = q_blk.shape[2] ** (-0.5)
    scores = (
        jnp.einsum("qhd,khd->hqk", q_blk, k_blk, preferred_element_type=jnp.float32) * score_scale
    )
    scores = scores + q_cum[:, :, None] - k_cum[:, None, :]
    q_pos = q_first + jnp.arange(q_blk.shape[0], dtype=jnp.int32)
    k_pos = k_first + jnp.arange(k_blk.shape[0], dtype=jnp.int32)
    allowed = k_pos[None, :] <= q_pos[:, None]
    scores = jnp.where(allowed[None], scores, -jnp.inf)
    block_top = jnp.max(scores, axis=-1)
    weights = jnp.exp(scores - block_top[..., None])
    block_total = jnp.sum(weights, axis=-1)
    block_out = jnp.einsum(
        "hqk,khd->hqd", weights.astype(jnp.bfloat16), v_blk, preferred_element_type=jnp.float32
    ).astype(jnp.bfloat16)
    return (block_top, block_total, block_out)


def merge_terms(state, terms):
    top_now, total_now, acc_now = state
    block_top, block_total, block_out = terms
    top_new = jnp.maximum(top_now, block_top)
    keep_old = jnp.exp(top_now - top_new)
    keep_new = jnp.exp(block_top - top_new)
    return (
        top_new,
        total_now * keep_old + block_total * keep_new,
        acc_now * keep_old[..., None] + block_out.astype(jnp.float32) * keep_new[..., None],
    )


def local(
    inputs,
    norm_gain,
    w_conv_in,
    w_conv_gate,
    conv_kernel,
    ln_gain,
    w_query,
    w_key,
    w_value,
    cum_gate,
    w_conv_out,
    w_attn_out,
):
    rows_here = inputs.shape[0]
    conv_width = w_conv_in.shape[0]
    attn_width = w_query.shape[0]
    heads_here = cum_gate.shape[0]
    head_dim = attn_width // heads_here
    taps_count = conv_kernel.shape[0]
    w_all = jnp.concatenate([w_conv_in, w_conv_gate, w_query, w_key, w_value], axis=0)
    gain_all = norm_gain.astype(jnp.float32)
    contract_dims = (((1,), (1,)), ((), ()))
    piece_f = gather_directly(inputs, "tp", 1).astype(jnp.float32)
    scaled_piece = (piece_f * gain_all[None, :]).astype(jnp.bfloat16)
    raw_proj = lax.dot_general(
        scaled_piece, w_all, contract_dims, preferred_element_type=jnp.float32
    )
    squares = jnp.sum(piece_f * piece_f, axis=1)
    rms = lax.rsqrt(squares / D + 1e-06)[:, None]
    proj = raw_proj * rms
    conv_in = proj[:, :conv_width]
    conv_gate = proj[:, conv_width : 2 * conv_width]
    query = proj[:, 2 * conv_width : 2 * conv_width + attn_width].astype(jnp.bfloat16)
    key_rows = proj[:, 2 * conv_width + attn_width : 2 * conv_width + 2 * attn_width].astype(
        jnp.bfloat16
    )
    value = proj[:, 2 * conv_width + 2 * attn_width :].astype(jnp.bfloat16)
    glu = (conv_in * jax.nn.sigmoid(conv_gate)).astype(jnp.bfloat16)
    rim_rows = passed_along(glu[rows_here - (taps_count - 1) :], "sp", 1)
    extended = jnp.concatenate([rim_rows, glu], axis=0)
    kernel = conv_kernel.astype(jnp.float32)
    conv_sum = jnp.zeros((rows_here, conv_width), jnp.float32)
    for tap_idx in range(taps_count):
        conv_sum = (
            conv_sum
            + extended[tap_idx : tap_idx + rows_here].astype(jnp.float32) * kernel[tap_idx][None, :]
        )
    chan_first, chan_second = lax.psum(
        (jnp.sum(conv_sum, axis=1), jnp.sum(conv_sum * conv_sum, axis=1)), "tp"
    )
    chan_mean = (chan_first / CONV_CH)[:, None]
    chan_var = (chan_second / CONV_CH)[:, None] - chan_mean * chan_mean
    normed = (
        (conv_sum - chan_mean) * lax.rsqrt(chan_var + 1e-05) * ln_gain.astype(jnp.float32)[None, :]
    )
    conv_out = jax.nn.silu(normed).astype(jnp.bfloat16)
    q_heads = query.reshape(rows_here, heads_here, head_dim)
    cum_all = lax.all_gather(cum_gate.T, "sp", axis=0, tiled=True)
    own_first = lax.axis_index("sp") * rows_here
    start_state = (
        jnp.full((heads_here, rows_here), neg_large, jnp.float32),
        jnp.zeros((heads_here, rows_here), jnp.float32),
        jnp.zeros((heads_here, rows_here, head_dim), jnp.float32),
    )
    state = start_state
    k_piece, v_piece = sent_together((key_rows, value), "sp", 0, 1)
    block_count = k_piece.shape[0] // rows_here
    k_split = k_piece.reshape(block_count, rows_here, heads_here, head_dim)
    v_split = v_piece.reshape(block_count, rows_here, heads_here, head_dim)

    def visit(carry, item):
        k_blk, v_blk, block_idx = item
        k_first = block_idx * rows_here
        k_cum = lax.dynamic_slice_in_dim(cum_all, k_first, rows_here, 0).T

        def take_block(inner):
            return merge_terms(
                inner, block_terms(q_heads, cum_gate, k_blk, v_blk, k_cum, own_first, k_first)
            )

        def skip_block(inner):
            return inner

        return (lax.cond(k_first <= own_first, take_block, skip_block, carry), None)

    state, unused = lax.scan(
        visit, state, (k_split, v_split, jnp.arange(block_count, dtype=jnp.int32))
    )
    top_all, total_all, acc_all = state
    attn_out = (
        (acc_all / total_all[..., None])
        .transpose(1, 0, 2)
        .reshape(rows_here, attn_width)
        .astype(jnp.bfloat16)
    )
    log_total = top_all + jnp.log(total_all)
    mixed = summed_on_arrival(
        (
            jnp.dot(conv_out, w_conv_out, preferred_element_type=jnp.float32)
            + jnp.dot(attn_out, w_attn_out, preferred_element_type=jnp.float32)
        ).astype(jnp.bfloat16),
        "tp",
        0,
    ).astype(jnp.bfloat16)
    return (mixed, log_total)


def solution(mesh):
    in_specs = (
        P(("grp", "sp"), "tp"),
        P(),
        P("tp", None),
        P("tp", None),
        P(None, "tp"),
        P("tp"),
        P("tp", None),
        P("tp", None),
        P("tp", None),
        P("tp", ("grp", "sp")),
        P("tp", None),
        P("tp", None),
    )
    out_specs = (P(("grp", "sp", "tp"), None), P("tp", ("grp", "sp")))
    return jax.shard_map(local, mesh=mesh, in_specs=in_specs, out_specs=out_specs, check_vma=False)
```

profile of v0, /device:TPU:2016, one launch (start us, length us, event | category | flops | bytes accessed | tf_op | source)
XLA Modules:
  0.0 345.3 jit_solution(744768911133563822)
XLA Ops:
  9.4 4.6 %all-to-all-start = ((bf16[8,256,256]{1,2,0:T(8,128)(2,1)}), bf16[8,256,256]{1,2,0:T(8,128)(2,1)S(1)}, u32[]{:S(2)}, u32[]{:S(2)}) async-start(bf16[8,256,256]{1,2,0:T(8,128)(2,1)} %broadcast_in_dim.25), calls=%async_computation | async-start | bytes 2097152 | tf_op jit(solution)/shard_map/all_to_all | solution.py:13
  18.3 11.6 %all-to-all-done = bf16[8,256,256]{1,2,0:T(8,128)(2,1)S(1)} async-done(((bf16[8,256,256]{1,2,0:T(8,128)(2,1)}), bf16[8,256,256]{1,2,0:T(8,128)(2,1)S(1)}, u32[]{:S(2)}, u32[]{:S(2)}) %all-to-all-start) | async-done | bytes 1048608 | tf_op jit(solution)/shard_map/all_to_all | solution.py:13
  30.6 2.8 fusion.62
  34.3 1.3 collective-permute-start
  35.6 53.0 %all_gather.6 = f32[8192,2]{0,1:T(2,128)S(1)} all-gather(f32[256,2]{0,1:T(2,128)S(1)} %bitcast.102), channel_id=1, replica_groups=mesh['grp'=2,'sp'=32,'tp'=8] {'sp'}, dimensions={0}, use_global_device_ids=true | all-gather | bytes 67584 | tf_op jit(solution)/shard_map/all_gather | solution.py:146
  89.5 12.5 %all-reduce = (f32[256]{0:T(256)S(1)}, f32[256]{0:T(256)S(1)}) all-reduce(f32[256]{0:T(256)S(1)} %get-tuple-element.184, f32[256]{0:T(256)S(1)} %get-tuple-element.183), channel_id=1, replica_groups=mesh['grp'=2,'sp'=32,'tp'=8] {'tp'}, use_global_device_ids=true, to_apply=%region_4.0 | all-reduce | flops 512 | bytes 4096 | tf_op jit(solution)/shard_map/psum | solution.py:136
  102.5 53.7 %all-gather.2.cloned.1.call-done = bf16[8192,256]{1,0:T(8,128)(2,1)} async-done(((bf16[256,256]{1,0:T(8,128)(2,1)}), bf16[8192,256]{1,0:T(8,128)(2,1)}) %all-gather.2.cloned.1.call-update) | async-done | bytes 4194320 | tf_op jit(solution)/shard_map/all_gather | solution.py:37
  156.1 4.5 %fusion.61 = (bf16[8192,128]{1,0:T(8,128)(2,1)}, bf16[8192,128]{1,0:T(8,128)(2,1)}) fusion(bf16[8192,256]{1,0:T(8,128)(2,1)} %all-gather.2.cloned.1.call-done), kind=kLoop, calls=%fused_computation.157 | loop fusion | bytes 8388608 | tf_op jit(solution)/shard_map/slice | solution.py:39
  160.6 8.2 %reshape.86 = bf16[32,256,2,64]{3,2,1,0:T(2,128)(2,1)} reshape(bf16[8192,128]{1,0:T(8,128)(2,1)} %get-tuple-element.218) | data formatting | bytes 4194304 | tf_op jit(solution)/shard_map/reshape | solution.py:157
  168.8 9.7 %copy.24 = bf16[32,256,2,64]{1,3,2,0:T(8,128)(2,1)} copy(bf16[32,256,2,64]{3,2,1,0:T(2,128)(2,1)} %reshape.86) | data formatting | bytes 4194304 | tf_op jit(solution)/shard_map/while | solution.py:174
  178.5 8.2 %reshape.85 = bf16[32,256,2,64]{3,2,1,0:T(2,128)(2,1)} reshape(bf16[8192,128]{1,0:T(8,128)(2,1)} %get-tuple-element.219) | data formatting | bytes 4194304 | tf_op jit(solution)/shard_map/reshape | solution.py:156
  186.7 9.8 %copy.23 = bf16[32,256,2,64]{1,3,2,0:T(8,128)(2,1)} copy(bf16[32,256,2,64]{3,2,1,0:T(2,128)(2,1)} %reshape.85) | data formatting | bytes 4194304 | tf_op jit(solution)/shard_map/while | solution.py:174
  196.5 119.1 %while.14 = (s32[]{:T(128)}, f32[2,256]{1,0:T(2,128)S(1)}, f32[2,256]{1,0:T(2,128)S(1)}, f32[2,256,64]{1,2,0:T(8,128)S(1)}, s32[32]{0:T(128)S(1)}, /*index=5*/s3...) while((s32[]{:T(128)}, f32[2,256]{1,0:T(2,128)S(1)}, ...), condition=%wide.region_10.11_spmd, body=%wide.region_5.10_spmd.sunk | while | flops 34966024 | bytes 2205049 | solution.py:174
  197.7 2.5 conditional.2
  197.9 1.2 fusion.60
  201.4 2.5 conditional.2
  201.6 1.2 fusion.60
  205.2 2.5 conditional.2
  205.3 1.2 fusion.60
  208.9 2.5 conditional.2
  209.0 1.2 fusion.60
  212.6 2.5 conditional.2
  212.8 1.2 fusion.60
  216.3 2.5 conditional.2
  216.5 1.2 fusion.60
  220.1 2.5 conditional.2
  220.2 1.2 fusion.60
  223.8 2.5 conditional.2
  223.9 1.2 fusion.60
  227.5 2.5 conditional.2
  227.6 1.2 fusion.60
  231.2 2.5 conditional.2
  231.4 1.2 fusion.60
  234.9 2.5 conditional.2
  235.1 1.2 fusion.60
  238.7 2.5 conditional.2
  238.8 1.2 fusion.60
  242.4 2.5 conditional.2
  242.5 1.2 fusion.60
  246.1 2.5 conditional.2
  246.3 1.2 fusion.60
  249.8 2.5 conditional.2
  250.0 1.2 fusion.60
  253.6 2.5 conditional.2
  253.7 1.2 fusion.60
  257.3 2.5 conditional.2
  261.0 2.5 conditional.2
  264.7 2.5 conditional.2
  268.4 2.5 conditional.2
  272.2 2.5 conditional.2
  275.9 2.5 conditional.2
  279.6 2.5 conditional.2
  283.3 2.5 conditional.2
  287.1 2.5 conditional.2
  290.8 2.5 conditional.2
  294.5 2.5 conditional.2
  298.2 2.5 conditional.2
  301.9 2.5 conditional.2
  305.7 2.5 conditional.2
  309.4 2.5 conditional.2
  313.1 2.5 conditional.2
  315.7 1.4 fusion.17
  317.1 4.5 %all-to-all-start.1 = ((bf16[8,32,2048]{2,1,0:T(8,128)(2,1)}), bf16[8,32,2048]{2,1,0:T(8,128)(2,1)S(1)}, u32[]{:S(2)}, u32[]{:S(2)}) async-start(bf16[8,32,2048]{2,1,0:T(8,128)(2,1)} %bitcast.99), calls=%async_computation.1 | async-start | bytes 2097152 | tf_op jit(solution)/shard_map/all_to_all | solution.py:52
  322.3 15.3 %all-to-all-done.1 = bf16[8,32,2048]{2,1,0:T(8,128)(2,1)S(1)} async-done(((bf16[8,32,2048]{2,1,0:T(8,128)(2,1)}), bf16[8,32,2048]{2,1,0:T(8,128)(2,1)S(1)}, u32[]{:S(2)}, u32[]{:S(2)}) %all-to-all-start.1) | async-done | bytes 1048608 | tf_op jit(solution)/shard_map/all_to_all | solution.py:52
  (295 shorter events, 90.2 us)
Async XLA Ops:
  7.2 94.8 %copy-start = (bf16[128,2048]{1,0:T(8,128)(2,1)S(1)}, bf16[128,2048]{1,0:T(8,128)(2,1)}, u32[]{:S(2)}) copy-start(bf16[128,2048]{1,0:T(8,128)(2,1)} %param.26) | copy-start | bytes 1572868
  7.2 6.9 %copy-start.8 = (bf16[2048]{0:T(1024)(128)(2,1)S(1)}, bf16[2048]{0:T(1024)(128)(2,1)}, u32[]{:S(2)}) copy-start(bf16[2048]{0:T(1024)(128)(2,1)} %param.17) | copy-start | bytes 12292
  7.2 6.9 %copy-start.2 = (bf16[128,2048]{1,0:T(8,128)(2,1)S(1)}, bf16[128,2048]{1,0:T(8,128)(2,1)}, u32[]{:S(2)}) copy-start(bf16[128,2048]{1,0:T(8,128)(2,1)} %param.18) | copy-start | bytes 1572868
  7.2 7.7 %copy-start.3 = (bf16[128,2048]{1,0:T(8,128)(2,1)S(1)}, bf16[128,2048]{1,0:T(8,128)(2,1)}, u32[]{:S(2)}) copy-start(bf16[128,2048]{1,0:T(8,128)(2,1)} %param.19) | copy-start | bytes 1572868
  8.3 7.5 %copy-start.4 = (bf16[128,2048]{1,0:T(8,128)(2,1)S(1)}, bf16[128,2048]{1,0:T(8,128)(2,1)}, u32[]{:S(2)}) copy-start(bf16[128,2048]{1,0:T(8,128)(2,1)} %param.22) | copy-start | bytes 1572868
  9.4 20.5 %all-to-all-start = ((bf16[8,256,256]{1,2,0:T(8,128)(2,1)}), bf16[8,256,256]{1,2,0:T(8,128)(2,1)S(1)}, u32[]{:S(2)}, u32[]{:S(2)}) async-start(bf16[8,256,256]{1,2,0:T(8,128)(2,1)} %broadcast_in_dim.25), calls=%async_computation | async-start | bytes 2097152 | tf_op jit(solution)/shard_map/all_to_all | solution.py:13
  14.0 142.1 %all-gather.2.cloned.1.call-start = ((), (), s32[]{:S(2)}) async-start(), calls=%async_computation.2 | async-start | bytes 4325376 | tf_op jit(solution)/shard_map/all_gather | solution.py:37
  14.1 2.6 copy-start.5
  14.1 3.4 copy-start.6
  30.6 3.6 %copy-start.7 = (bf16[31,128]{1,0:T(8,128)(2,1)S(1)}, bf16[31,128]{1,0:T(8,128)(2,1)}, u32[]{:S(2)}) copy-start(bf16[31,128]{1,0:T(8,128)(2,1)} %param.20) | copy-start | bytes 23812
  30.6 5.0 %copy-start.9 = (f32[2,256]{1,0:T(2,128)S(1)}, f32[2,256]{1,0:T(2,128)}, u32[]{:S(2)}) copy-start(f32[2,256]{1,0:T(2,128)} %param.25) | copy-start | bytes 6148
  30.6 58.0 %copy-start.10 = (bf16[128]{0:T(256)(128)(2,1)S(1)}, bf16[128]{0:T(256)(128)(2,1)}, u32[]{:S(2)}) copy-start(bf16[128]{0:T(256)(128)(2,1)} %param.21) | copy-start | bytes 772
  34.3 54.5 %collective-permute-start = (bf16[30,128]{1,0:T(8,128)(2,1)S(1)}, bf16[30,128]{1,0:T(8,128)(2,1)S(1)}, u32[]{:S(2)}, u32[]{:S(2)}) collective-permute-start(bf16[30,128]{1,0:T(8,128)(2,1)S(1)} %slice.282), channel_id=1, source_target_pairs={{0,8},{8,16},{16,24},{24,32},{32,40},{40,48},{48,56},{56,64},{64,7... | collective-permute-start | bytes 23048 | tf_op jit(solution)/shard_map/ppermute | solution.py:32
  196.5 119.2 %copy-start.1 = (bf16[128,2048]{1,0:T(8,128)(2,1)S(1)}, bf16[128,2048]{1,0:T(8,128)(2,1)}, u32[]{:S(2)}) copy-start(bf16[128,2048]{1,0:T(8,128)(2,1)} %param.27) | copy-start | bytes 1572868
  317.1 20.5 %all-to-all-start.1 = ((bf16[8,32,2048]{2,1,0:T(8,128)(2,1)}), bf16[8,32,2048]{2,1,0:T(8,128)(2,1)S(1)}, u32[]{:S(2)}, u32[]{:S(2)}) async-start(bf16[8,32,2048]{2,1,0:T(8,128)(2,1)} %bitcast.99), calls=%async_computation.1 | async-start | bytes 2097152 | tf_op jit(solution)/shard_map/all_to_all | solution.py:52
Sparse Core Ops, SparseCore 0:
  34.3 121.7 all-gather.1
where the time goes:
time: 349 us; the launch traced here: 345 us
  waiting for transfers between devices  80.7 us (23%)
  matrix products  76.5 us (22%)
  local copies, waits for them, and re-layouts  66.7 us (19%)
  blocking collectives  65.5 us (19%)
  loops' own time  21.1 us (6%)
  between operations  14.3 us (4%)
  starting transfers between devices  10.5 us (3%)
  other arithmetic  10 us (3%)
    all_gather x1, waiting for transfers between devices, sent_together(): filled, at, outs = (lax.all_gather(both, axis, axis=dim, tiled=True), 0, [])  53.7 us
    all_gather x1, blocking collectives, local(): cum_all = lax.all_gather(cum_gate.T, 'sp', axis=0, tiled=True)  53 us
    dot_general x32, matrix products, block_terms(): jnp.einsum('qhd,khd->hqk', q_blk, k_blk, preferred_element_type=jnp.float32)  37.2 us
    dot_general x32, matrix products, block_terms(): jnp.einsum('hqk,khd->hqd', weights.astype(jnp.bfloat16), v_blk, preferred...  34.5 us
    another operation x1, loops' own time, local(): lax.scan(visit, state, (k_split, v_split, jnp.arange(block_count, dtype=j...  19.5 us
    while x2, local copies, waits for them, and re-layouts, local(): lax.scan(visit, state, (k_split, v_split, jnp.arange(block_count, dtype=j...  19.5 us
    dynamic_slice x32, local copies, waits for them, and re-layouts, local(): lax.scan(visit, state, (k_split, v_split, jnp.arange(block_count, dtype=j...  18.8 us
    all_to_all x1, waiting for transfers between devices, summed_on_arrival(): lax.all_to_all(in_blocks(shard, dim, devices), axis, 0, 0, tiled=True)  15.3 us
  transfers between devices with their start and end apart: 4, of which 3 were waited for; matrix products, arithmetic and copies ran while one was open for 2% of the time, Pallas kernels for 0%

commit v1 on v0

--- a/solution.py
+++ b/solution.py
@@ -143,7 +143,9 @@
     )
     conv_out = jax.nn.silu(normed).astype(jnp.bfloat16)
     q_heads = query.reshape(rows_here, heads_here, head_dim)
-    cum_all = lax.all_gather(cum_gate.T, "sp", axis=0, tiled=True)
+    cum_all = jnp.concatenate(
+        lax.all_to_all(jnp.stack([cum_gate.T] * lax.axis_size("sp"), 0), "sp", 0, 0), 0
+    )
     own_first = lax.axis_index("sp") * rows_here
     start_state = (
         jnp.full((heads_here, rows_here), neg_large, jnp.float32),

time: 349 us -> 353 us (1.011)
  blocking collectives: 65.5 us -> 13.1 us
  waiting for transfers between devices: 80.7 us -> 129 us
  starting transfers between devices: 10.5 us -> 14.9 us
    all_gather x1 -> x0, blocking collectives: 53 us -> none  [local(): cum_all = lax.all_gather(cum_gate.T, 'sp', axis=0, tiled=True)]
    all_gather x1, waiting for transfers between devices: 53.7 us -> 98.2 us  [sent_together(): filled, at, outs = (lax.all_gather(both, axis, axis=dim, tiled=True), 0, [])]
    all_to_all x0 -> x1, starting transfers between devices: none -> 5.16 us  [local(): lax.all_to_all(jnp.stack([cum_gate.T] * lax.axis_size('sp'), 0), 'sp', 0, 0)]
    ppermute x1, waiting for transfers between devices: 0.01 us -> 4.08 us  [passed_along(): return lax.ppermute(block, axis, route)]
  transfers between devices with their start and end apart: 4 -> 5, of which waited for: 3 -> 4; matrix products, arithmetic and copies ran while one was open for 2% -> 14% of each run, Pallas kernels for 0% -> 0%
where the time goes in v1:
time: 353 us; the launch traced here: 349 us
  waiting for transfers between devices  129 us (37%)
  matrix products  76.6 us (22%)
  local copies, waits for them, and re-layouts  67.8 us (19%)
  loops' own time  22.9 us (6%)
  starting transfers between devices  14.9 us (4%)
  between operations  14.4 us (4%)
  blocking collectives  13.1 us (4%)
  other arithmetic  10 us (3%)
    all_gather x1, waiting for transfers between devices, sent_together(): filled, at, outs = (lax.all_gather(both, axis, axis=dim, tiled=True), 0, [])  98.2 us
    dot_general x32, matrix products, block_terms(): jnp.einsum('qhd,khd->hqk', q_blk, k_blk, preferred_element_type=jnp.float32)  37.2 us
    dot_general x32, matrix products, block_terms(): jnp.einsum('hqk,khd->hqd', weights.astype(jnp.bfloat16), v_blk, preferred...  34.6 us
    another operation x1, loops' own time, local(): lax.scan(visit, state, (k_split, v_split, jnp.arange(block_count, dtype=j...  21.4 us
    while x2, local copies, waits for them, and re-layouts, local(): lax.scan(visit, state, (k_split, v_split, jnp.arange(block_count, dtype=j...  19.5 us
    dynamic_slice x32, local copies, waits for them, and re-layouts, local(): lax.scan(visit, state, (k_split, v_split, jnp.arange(block_count, dtype=j...  19.3 us
    all_to_all x1, waiting for transfers between devices, summed_on_arrival(): lax.all_to_all(in_blocks(shard, dim, devices), axis, 0, 0, tiled=True)  15.1 us
    psum x1, blocking collectives, local(): lax.psum((jnp.sum(conv_sum, axis=1), jnp.sum(conv_sum * conv_sum, axis=1)...  13.1 us
  transfers between devices with their start and end apart: 5, of which 4 were waited for; matrix products, arithmetic and copies ran while one was open for 14% of the time, Pallas kernels for 0%

profile of v1, /device:TPU:2016, one launch (start us, length us, event | category | flops | bytes accessed | tf_op | source)
XLA Modules:
  0.0 348.7 jit_solution(16665642750519962649)
XLA Ops:
  9.4 4.6 %all-to-all-start = ((bf16[8,256,256]{1,2,0:T(8,128)(2,1)}), bf16[8,256,256]{1,2,0:T(8,128)(2,1)S(1)}, u32[]{:S(2)}, u32[]{:S(2)}) async-start(bf16[8,256,256]{1,2,0:T(8,128)(2,1)} %broadcast_in_dim.25), calls=%async_computation | async-start | bytes 2097152 | tf_op jit(solution)/shard_map/all_to_all | solution.py:13
  18.3 11.6 %all-to-all-done = bf16[8,256,256]{1,2,0:T(8,128)(2,1)S(1)} async-done(((bf16[8,256,256]{1,2,0:T(8,128)(2,1)}), bf16[8,256,256]{1,2,0:T(8,128)(2,1)S(1)}, u32[]{:S(2)}, u32[]{:S(2)}) %all-to-all-start) | async-done | bytes 1048608 | tf_op jit(solution)/shard_map/all_to_all | solution.py:13
  30.6 2.8 fusion.62
  34.8 5.2 %all-to-all-start.1 = ((f32[32,256,2]{1,2,0:T(2,128)}), f32[32,256,2]{1,2,0:T(2,128)S(1)}, u32[]{:S(2)}, u32[]{:S(2)}) async-start(f32[32,256,2]{1,2,0:T(2,128)} %stack.2), calls=%async_computation.1 | async-start | bytes 131072 | tf_op jit(solution)/shard_map/all_to_all | solution.py:147
  40.1 1.3 collective-permute-start
  41.6 4.1 %collective-permute-done = bf16[30,128]{1,0:T(8,128)(2,1)S(1)} collective-permute-done((bf16[30,128]{1,0:T(8,128)(2,1)S(1)}, bf16[30,128]{1,0:T(8,128)(2,1)S(1)}, u32[]{:S(2)}, u32[]{:S(2)}) %collective-permute-start) | collective-permute-done | bytes 7712 | tf_op jit(solution)/shard_map/ppermute | solution.py:32
  46.3 13.1 %all-reduce = (f32[256]{0:T(256)S(1)}, f32[256]{0:T(256)S(1)}) all-reduce(f32[256]{0:T(256)S(1)} %get-tuple-element.195, f32[256]{0:T(256)S(1)} %get-tuple-element.194), channel_id=1, replica_groups=mesh['grp'=2,'sp'=32,'tp'=8] {'tp'}, use_global_device_ids=true, to_apply=%region_4.0 | all-reduce | flops 512 | bytes 4096 | tf_op jit(solution)/shard_map/psum | solution.py:136
  59.9 98.2 %all-gather.2.cloned.1.call-done = bf16[8192,256]{1,0:T(8,128)(2,1)} async-done(((bf16[256,256]{1,0:T(8,128)(2,1)}), bf16[8192,256]{1,0:T(8,128)(2,1)}) %all-gather.2.cloned.1.call-update) | async-done | bytes 4194320 | tf_op jit(solution)/shard_map/all_gather | solution.py:37
  158.1 4.5 %fusion.61 = (bf16[8192,128]{1,0:T(8,128)(2,1)}, bf16[8192,128]{1,0:T(8,128)(2,1)}) fusion(bf16[8192,256]{1,0:T(8,128)(2,1)} %all-gather.2.cloned.1.call-done), kind=kLoop, calls=%fused_computation.157 | loop fusion | bytes 8388608 | tf_op jit(solution)/shard_map/slice | solution.py:39
  162.6 8.2 %reshape.92 = bf16[32,256,2,64]{3,2,1,0:T(2,128)(2,1)} reshape(bf16[8192,128]{1,0:T(8,128)(2,1)} %get-tuple-element.229) | data formatting | bytes 4194304 | tf_op jit(solution)/shard_map/reshape | solution.py:159
  170.8 9.7 %copy.31 = bf16[32,256,2,64]{1,3,2,0:T(8,128)(2,1)} copy(bf16[32,256,2,64]{3,2,1,0:T(2,128)(2,1)} %reshape.92) | data formatting | bytes 4194304 | tf_op jit(solution)/shard_map/while | solution.py:176
  180.5 8.2 %reshape.91 = bf16[32,256,2,64]{3,2,1,0:T(2,128)(2,1)} reshape(bf16[8192,128]{1,0:T(8,128)(2,1)} %get-tuple-element.230) | data formatting | bytes 4194304 | tf_op jit(solution)/shard_map/reshape | solution.py:158
  188.7 9.7 %copy.30 = bf16[32,256,2,64]{1,3,2,0:T(8,128)(2,1)} copy(bf16[32,256,2,64]{3,2,1,0:T(2,128)(2,1)} %reshape.91) | data formatting | bytes 4194304 | tf_op jit(solution)/shard_map/while | solution.py:176
  198.5 121.5 %while.14 = (s32[]{:T(128)}, f32[2,256]{1,0:T(2,128)S(1)}, f32[2,256]{1,0:T(2,128)S(1)}, f32[2,256,64]{1,2,0:T(8,128)S(1)}, s32[32]{0:T(128)S(1)}, /*index=5*/s3...) while((s32[]{:T(128)}, f32[2,256]{1,0:T(2,128)S(1)}, ...), condition=%wide.region_10.11_spmd, body=%wide.region_5.10_spmd.sunk | while | flops 34966024 | bytes 2205049 | solution.py:176
  199.8 2.5 conditional.2
  199.9 1.2 fusion.60
  203.6 2.5 conditional.2
  203.7 1.2 fusion.60
  207.4 2.5 conditional.2
  207.5 1.2 fusion.60
  211.2 2.5 conditional.2
  215.0 2.5 conditional.2
  218.8 2.5 conditional.2
  218.9 1.2 fusion.60
  222.5 2.5 conditional.2
  222.7 1.2 fusion.60
  226.3 2.5 conditional.2
  230.1 2.5 conditional.2
  233.9 2.5 conditional.2
  234.1 1.2 fusion.60
  237.7 2.5 conditional.2
  237.9 1.2 fusion.60
  241.5 2.5 conditional.2
  245.3 2.5 conditional.2
  245.5 1.2 fusion.60
  249.1 2.5 conditional.2
  249.3 1.2 fusion.60
  252.9 2.5 conditional.2
  253.1 1.2 fusion.60
  256.7 2.5 conditional.2
  260.5 2.5 conditional.2
  260.7 1.2 fusion.60
  264.3 2.5 conditional.2
  264.5 1.2 fusion.60
  268.1 2.5 conditional.2
  271.9 2.5 conditional.2
  275.7 2.5 conditional.2
  275.9 1.2 fusion.60
  279.5 2.5 conditional.2
  279.7 1.2 fusion.60
  283.3 2.5 conditional.2
  287.1 2.5 conditional.2
  290.9 2.5 conditional.2
  291.1 1.2 fusion.60
  294.7 2.5 conditional.2
  298.5 2.5 conditional.2
  302.3 2.5 conditional.2
  306.1 2.5 conditional.2
  309.9 2.5 conditional.2
  313.7 2.5 conditional.2
  317.5 2.5 conditional.2
  320.1 1.4 fusion.17
  321.5 3.8 %all-to-all-start.2 = ((bf16[8,32,2048]{2,1,0:T(8,128)(2,1)}), bf16[8,32,2048]{2,1,0:T(8,128)(2,1)S(1)}, u32[]{:S(2)}, u32[]{:S(2)}) async-start(bf16[8,32,2048]{2,1,0:T(8,128)(2,1)} %bitcast.100), calls=%async_computation.2 | async-start | bytes 2097152 | tf_op jit(solution)/shard_map/all_to_all | solution.py:52
  325.9 15.1 %all-to-all-done.2 = bf16[8,32,2048]{2,1,0:T(8,128)(2,1)S(1)} async-done(((bf16[8,32,2048]{2,1,0:T(8,128)(2,1)}), bf16[8,32,2048]{2,1,0:T(8,128)(2,1)S(1)}, u32[]{:S(2)}, u32[]{:S(2)}) %all-to-all-start.2) | async-done | bytes 1048608 | tf_op jit(solution)/shard_map/all_to_all | solution.py:52
  (297 shorter events, 92.5 us)
Async XLA Ops:
  7.2 52.2 %copy-start = (bf16[128,2048]{1,0:T(8,128)(2,1)S(1)}, bf16[128,2048]{1,0:T(8,128)(2,1)}, u32[]{:S(2)}) copy-start(bf16[128,2048]{1,0:T(8,128)(2,1)} %param.26) | copy-start | bytes 1572868
  7.2 6.9 %copy-start.8 = (bf16[2048]{0:T(1024)(128)(2,1)S(1)}, bf16[2048]{0:T(1024)(128)(2,1)}, u32[]{:S(2)}) copy-start(bf16[2048]{0:T(1024)(128)(2,1)} %param.17) | copy-start | bytes 12292
  7.2 6.9 %copy-start.2 = (bf16[128,2048]{1,0:T(8,128)(2,1)S(1)}, bf16[128,2048]{1,0:T(8,128)(2,1)}, u32[]{:S(2)}) copy-start(bf16[128,2048]{1,0:T(8,128)(2,1)} %param.18) | copy-start | bytes 1572868
  7.2 7.7 %copy-start.3 = (bf16[128,2048]{1,0:T(8,128)(2,1)S(1)}, bf16[128,2048]{1,0:T(8,128)(2,1)}, u32[]{:S(2)}) copy-start(bf16[128,2048]{1,0:T(8,128)(2,1)} %param.19) | copy-start | bytes 1572868
  8.3 7.4 %copy-start.4 = (bf16[128,2048]{1,0:T(8,128)(2,1)S(1)}, bf16[128,2048]{1,0:T(8,128)(2,1)}, u32[]{:S(2)}) copy-start(bf16[128,2048]{1,0:T(8,128)(2,1)} %param.22) | copy-start | bytes 1572868
  9.4 20.5 %all-to-all-start = ((bf16[8,256,256]{1,2,0:T(8,128)(2,1)}), bf16[8,256,256]{1,2,0:T(8,128)(2,1)S(1)}, u32[]{:S(2)}, u32[]{:S(2)}) async-start(bf16[8,256,256]{1,2,0:T(8,128)(2,1)} %broadcast_in_dim.25), calls=%async_computation | async-start | bytes 2097152 | tf_op jit(solution)/shard_map/all_to_all | solution.py:13
  14.0 144.1 %all-gather.2.cloned.1.call-start = ((), (), s32[]{:S(2)}) async-start(), calls=%async_computation.3 | async-start | bytes 4325376 | tf_op jit(solution)/shard_map/all_gather | solution.py:37
  14.1 2.6 copy-start.5
  14.1 3.4 copy-start.6
  30.6 3.6 %copy-start.9 = (f32[2,256]{1,0:T(2,128)S(1)}, f32[2,256]{1,0:T(2,128)}, u32[]{:S(2)}) copy-start(f32[2,256]{1,0:T(2,128)} %param.25) | copy-start | bytes 6148
  30.6 9.4 %copy-start.7 = (bf16[31,128]{1,0:T(8,128)(2,1)S(1)}, bf16[31,128]{1,0:T(8,128)(2,1)}, u32[]{:S(2)}) copy-start(bf16[31,128]{1,0:T(8,128)(2,1)} %param.20) | copy-start | bytes 23812
  30.6 10.8 %copy-start.10 = (bf16[128]{0:T(256)(128)(2,1)S(1)}, bf16[128]{0:T(256)(128)(2,1)}, u32[]{:S(2)}) copy-start(bf16[128]{0:T(256)(128)(2,1)} %param.21) | copy-start | bytes 772
  34.8 163.6 %all-to-all-start.1 = ((f32[32,256,2]{1,2,0:T(2,128)}), f32[32,256,2]{1,2,0:T(2,128)S(1)}, u32[]{:S(2)}, u32[]{:S(2)}) async-start(f32[32,256,2]{1,2,0:T(2,128)} %stack.2), calls=%async_computation.1 | async-start | bytes 131072 | tf_op jit(solution)/shard_map/all_to_all | solution.py:147
  40.1 5.6 %collective-permute-start = (bf16[30,128]{1,0:T(8,128)(2,1)S(1)}, bf16[30,128]{1,0:T(8,128)(2,1)S(1)}, u32[]{:S(2)}, u32[]{:S(2)}) collective-permute-start(bf16[30,128]{1,0:T(8,128)(2,1)S(1)} %slice.282), channel_id=1, source_target_pairs={{0,8},{8,16},{16,24},{24,32},{32,40},{40,48},{48,56},{56,64},{64,7... | collective-permute-start | bytes 23048 | tf_op jit(solution)/shard_map/ppermute | solution.py:32
  198.5 121.6 %copy-start.1 = (bf16[128,2048]{1,0:T(8,128)(2,1)S(1)}, bf16[128,2048]{1,0:T(8,128)(2,1)}, u32[]{:S(2)}) copy-start(bf16[128,2048]{1,0:T(8,128)(2,1)} %param.27) | copy-start | bytes 1572868
  321.5 19.5 %all-to-all-start.2 = ((bf16[8,32,2048]{2,1,0:T(8,128)(2,1)}), bf16[8,32,2048]{2,1,0:T(8,128)(2,1)S(1)}, u32[]{:S(2)}, u32[]{:S(2)}) async-start(bf16[8,32,2048]{2,1,0:T(8,128)(2,1)} %bitcast.100), calls=%async_computation.2 | async-start | bytes 2097152 | tf_op jit(solution)/shard_map/all_to_all | solution.py:52
Sparse Core Ops, SparseCore 0:
  34.3 123.7 all-gather.1
